TPU v7x, 32 devices: a whole 2x2x4 slice. The times are simulated.
32 devices in a mesh: sp: 4 (over z), tp: 4 (over y, x), dp: 2 (over core).
Axes of the slice: x: 2, y: 2, z: 4, core: 2. Of those that a mesh axis runs over, the one named last changes fastest.
Arguments:
- latent_in: bfloat16 [3072, 2048], P(('dp', 'sp', 'tp')), parts along dimension 0, may hold values from -6 to 6
- condition: bfloat16 [4096], P(('dp', 'sp')), parts along dimension 0, may hold values from -8 to 8
- context_latent: bfloat16 [1024, 256], P(('dp', 'sp')), parts along dimension 0, may hold values from -6 to 6
- context_rope: bfloat16 [1024, 64], P(('dp', 'sp')), parts along dimension 0, may hold values from -6 to 6
- shift_weight: bfloat16 [2048, 2048], P('sp', 'tp'), may hold values from -0.125 to 0.125
- scale_weight: bfloat16 [2048, 2048], P('sp', 'tp'), may hold values from -0.125 to 0.125
- gate_weight: bfloat16 [2048, 2048], P('sp', 'tp'), may hold values from -0.125 to 0.125
- norm_gain: float32 [2048], replicated, may hold values from 0.1 to 1.9
- down_query: bfloat16 [2048, 512], replicated, may hold values from -0.125 to 0.125
- down_latent: bfloat16 [2048, 256], replicated, may hold values from -0.125 to 0.125
- down_rope: bfloat16 [2048, 64], replicated, may hold values from -0.125 to 0.125
- query_gain: float32 [512], replicated, may hold values from 0.5 to 60
- latent_gain: float32 [256], replicated, may hold values from 0.1 to 1.9
- up_query: bfloat16 [512, 1536], P(None, 'tp'), may hold values from -0.25 to 0.25
- up_key: bfloat16 [256, 1024], P(None, 'tp'), may hold values from -0.375 to 0.375
- up_value: bfloat16 [256, 1024], P(None, 'tp'), may hold values from -0.375 to 0.375
- context_bias: float32 [8], P('tp'), may hold values from 1 to 2.5
- out_weight: bfloat16 [1024, 2048], replicated, may hold values from -3 to 3
Outputs:
- mixed_out: bfloat16 [3072, 2048], P(('dp', 'sp', 'tp')), parts along dimension 0
There are 2 independent parts, one for each index of `dp`. A program takes and returns all parts, laid end to end along the dimension named above; an argument that names none is the same for every part. Nothing has to cross between parts.
All inputs are finite; a program needn't handle non-finite values.
Results may differ from a plain program's by a relative error of at most 0.039.
The roundings to bfloat16 on the way count: a program that leaves them out, or rounds other values in their place, can miss the bound.
Values may be sent and summed in bfloat16 or wider, within the bound.
A program may use at most 128 MiB of HBM per device.

v0:
```python
import jax
import jax.numpy as jnp
from jax import lax
from jax.sharding import PartitionSpec as P

QK_NOPE = 128
QK_ROPE = 64
V_HEAD = 128
GRID_W = 64
epsilon = 1e-06
rope_base = 10000.0
block_limit = 2048


def rms_scaled(values, gain_vec):
    mean_sq = jnp.mean(values * values, axis=-1, keepdims=True)
    return values * lax.rsqrt(mean_sq + epsilon) * gain_vec


def rope_tables(positions, rope_width):
    freq_count = rope_width // 4
    inverse = rope_base ** (-jnp.arange(freq_count, dtype=jnp.float32) / freq_count)
    grid_row = (positions // GRID_W).astype(jnp.float32)
    grid_col = (positions % GRID_W).astype(jnp.float32)
    row_angle = grid_row[:, None] * inverse
    col_angle = grid_col[:, None] * inverse
    angles = jnp.concatenate([row_angle, row_angle, col_angle, col_angle], axis=-1)
    return (jnp.cos(angles), jnp.sin(angles))


def rope_turn(values, cosine_table, sine_table):
    part_one, part_two, part_three, part_four = jnp.split(values, 4, axis=-1)
    turned = jnp.concatenate([-part_two, part_one, -part_four, part_three], axis=-1)
    return values * cosine_table + turned * sine_table


def attend(attn_state, query_nope, query_rope, keys_nope, values_in, keys_rope, bias_col):
    score_scale = (query_nope.shape[-1] + query_rope.shape[-1]) ** (-0.5)
    scores = jnp.einsum("thd,khd->htk", query_nope, keys_nope, preferred_element_type=jnp.float32)
    scores = scores + jnp.einsum(
        "thr,kr->htk", query_rope, keys_rope, preferred_element_type=jnp.float32
    )
    scores = scores * score_scale + bias_col
    run_max, run_total, run_acc = attn_state
    new_max = jnp.maximum(run_max, jnp.max(scores, axis=-1))
    shrink = jnp.exp(run_max - new_max)
    weights = jnp.exp(scores - new_max[:, :, None])
    new_total = run_total * shrink + jnp.sum(weights, axis=-1)
    new_acc = run_acc * shrink[:, :, None] + jnp.einsum(
        "htk,khd->htd", weights.astype(jnp.bfloat16), values_in, preferred_element_type=jnp.float32
    )
    return (new_max, new_total, new_acc)


def over_blocks(attn_state, arrays, handle):
    row_count = arrays[0].shape[0]
    block_rows = 1
    for candidate in range(min(row_count, block_limit), 0, -1):
        if row_count % candidate == 0:
            block_rows = candidate
            break
    block_count = row_count // block_rows
    if block_count == 1:
        return handle(attn_state, arrays)
    stacked = tuple(
        (array_in.reshape((block_count, block_rows) + array_in.shape[1:]) for array_in in arrays)
    )

    def one_turn(inner_state, pieces):
        return (handle(inner_state, pieces), None)

    return lax.scan(one_turn, attn_state, stacked)[0]


def on_device(
    latent_in,
    condition,
    context_latent,
    context_rope,
    shift_weight,
    scale_weight,
    gate_weight,
    norm_gain,
    down_query,
    down_latent,
    down_rope,
    query_gain,
    latent_gain,
    up_query,
    up_key,
    up_value,
    context_bias,
    out_weight,
):
    activated = jax.nn.silu(condition.astype(jnp.float32)).astype(jnp.bfloat16)
    partials = jnp.stack(
        [
            jnp.dot(activated, weight_in, preferred_element_type=jnp.float32)
            for weight_in in (shift_weight, scale_weight, gate_weight)
        ]
    )
    summed = lax.psum(partials, "sp")
    modulation = lax.all_gather(summed, "tp", axis=1, tiled=True)
    shift_vec = modulation[0]
    scale_vec = modulation[1]
    gate_vec = modulation[2]
    residual_in = latent_in.astype(jnp.float32)
    normed = (rms_scaled(residual_in, norm_gain) * (1.0 + scale_vec) + shift_vec).astype(
        jnp.bfloat16
    )
    query_low = rms_scaled(
        jnp.dot(normed, down_query, preferred_element_type=jnp.float32), query_gain
    ).astype(jnp.bfloat16)
    latent_low = rms_scaled(
        jnp.dot(normed, down_latent, preferred_element_type=jnp.float32), latent_gain
    ).astype(jnp.bfloat16)
    local_rows = latent_in.shape[0]
    first_row = (lax.axis_index("sp") * lax.axis_size("tp") + lax.axis_index("tp")) * local_rows
    own_positions = first_row + jnp.arange(local_rows, dtype=jnp.int32)
    own_cosine, own_sine = rope_tables(own_positions, QK_ROPE)
    rope_keys = rope_turn(
        jnp.dot(normed, down_rope, preferred_element_type=jnp.float32), own_cosine, own_sine
    ).astype(jnp.bfloat16)
    query_group, latent_group, rope_group = (
        lax.all_gather(query_low, "tp", axis=0, tiled=True),
        lax.all_gather(latent_low, "tp", axis=0, tiled=True),
        lax.all_gather(rope_keys, "tp", axis=0, tiled=True),
    )
    group_rows = query_group.shape[0]
    group_positions = lax.axis_index("sp") * group_rows + jnp.arange(group_rows, dtype=jnp.int32)
    group_cosine, group_sine = rope_tables(group_positions, QK_ROPE)
    head_count = up_key.shape[1] // QK_NOPE
    queries = jnp.dot(query_group, up_query, preferred_element_type=jnp.float32).reshape(
        group_rows, head_count, QK_NOPE + QK_ROPE
    )
    query_nope = queries[:, :, :QK_NOPE].astype(jnp.bfloat16)
    query_rope = rope_turn(
        queries[:, :, QK_NOPE:], group_cosine[:, None, :], group_sine[:, None, :]
    ).astype(jnp.bfloat16)
    context_all, context_keys_rope = (
        lax.all_gather(context_latent, "sp", axis=0, tiled=True),
        lax.all_gather(context_rope, "sp", axis=0, tiled=True),
    )
    context_count = context_all.shape[0]
    context_nope = (
        jnp.dot(context_all, up_key, preferred_element_type=jnp.float32)
        .astype(jnp.bfloat16)
        .reshape(context_count, head_count, QK_NOPE)
    )
    context_values = (
        jnp.dot(context_all, up_value, preferred_element_type=jnp.float32)
        .astype(jnp.bfloat16)
        .reshape(context_count, head_count, V_HEAD)
    )
    start_state = (
        jnp.full((head_count, group_rows), -jnp.inf, jnp.float32),
        jnp.zeros((head_count, group_rows), jnp.float32),
        jnp.zeros((head_count, group_rows, V_HEAD), jnp.float32),
    )
    bias_col = context_bias[:, None, None]

    def context_step(inner_state, pieces):
        return attend(
            inner_state, query_nope, query_rope, pieces[0], pieces[1], pieces[2], bias_col
        )

    attn_state = over_blocks(
        start_state, (context_nope, context_values, context_keys_rope), context_step
    )
    own_nope = jnp.dot(latent_group, up_key, preferred_element_type=jnp.float32).astype(
        jnp.bfloat16
    )
    own_values = jnp.dot(latent_group, up_value, preferred_element_type=jnp.float32).astype(
        jnp.bfloat16
    )

    def expanded_step(inner_state, pieces):
        piece_rows = pieces[0].shape[0]
        return attend(
            inner_state,
            query_nope,
            query_rope,
            pieces[0].reshape(piece_rows, head_count, QK_NOPE),
            pieces[1].reshape(piece_rows, head_count, V_HEAD),
            pieces[2],
            0.0,
        )

    attn_state = over_blocks(
        attn_state,
        (
            lax.all_gather(own_nope, "sp", axis=0, tiled=True),
            lax.all_gather(own_values, "sp", axis=0, tiled=True),
            lax.all_gather(rope_group, "sp", axis=0, tiled=True),
        ),
        expanded_step,
    )
    attended = (attn_state[2] / attn_state[1][:, :, None]).astype(jnp.bfloat16)
    attended = attended.transpose(1, 0, 2).reshape(group_rows, head_count * V_HEAD)
    token_major = lax.all_to_all(attended, "tp", split_axis=0, concat_axis=1, tiled=True)
    mixed = jnp.dot(token_major, out_weight, preferred_element_type=jnp.float32)
    return (residual_in + gate_vec * mixed).astype(jnp.bfloat16)


def solution(mesh):
    in_specs = (
        P(("dp", "sp", "tp"), None),
        P(("dp", "sp")),
        P(("dp", "sp"), None),
        P(("dp", "sp"), None),
        P("sp", "tp"),
        P("sp", "tp"),
        P("sp", "tp"),
        P(),
        P(),
        P(),
        P(),
        P(),
        P(),
        P(None, "tp"),
        P(None, "tp"),
        P(None, "tp"),
        P("tp"),
        P(),
    )
    out_specs = P(("dp", "sp", "tp"), None)
    return jax.shard_map(
        on_device, mesh=mesh, in_specs=in_specs, out_specs=out_specs, check_vma=False
    )
```

profile of v0, /device:TPU:0, one launch (start us, length us, event | category | flops | bytes accessed | tf_op | source)
XLA Modules:
  0.0 158.6 jit_solution(2897633564219635338)
XLA Ops:
  1.3 1.2 fusion.72
  2.6 1.2 fusion.73
  3.8 1.3 fusion.74
  5.1 13.8 %psum.7 = f32[3,512]{1,0:T(4,128)S(1)} all-reduce(f32[3,512]{1,0:T(4,128)S(1)} %pad_maximum_fusion.2), channel_id=1, replica_groups=mesh['sp'=4,'tp'=4,'dp'=2] {'sp'}, use_global_device_ids=true, to_apply=%region_0.1 | all-reduce | flops 1536 | bytes 12288 | tf_op jit(solution)/shard_map/psum | solution.py:102
  18.9 8.2 %all_gather.27 = f32[3,2048]{1,0:T(4,128)S(1)} all-gather(f32[3,512]{1,0:T(4,128)S(1)} %psum.7), channel_id=1, replica_groups=mesh['sp'=4,'tp'=4,'dp'=2] {'tp'}, dimensions={1}, use_global_device_ids=true | all-gather | bytes 30720 | tf_op jit(solution)/shard_map/all_gather | solution.py:103
  27.1 1.2 fusion.26
  28.4 1.9 %multiply_reduce_fusion.1 = (f32[96]{0:T(128)S(1)}, f32[96,256]{1,0:T(8,128)S(1)}) fusion(bf16[2048,256]{1,0:T(8,128)(2,1)} %param.27, bf16[96,2048]{1,0:T(8,128)(2,1)} %param.18, f32[2048]{0:T(1024)S(1)} %bitcast.119, f32[2048]{0:T(1024)S(1)} %bitcast.122, f32[2048]{0:T(1024)} %param.25, f32[96]{0:T(128)S(1)} %add_rsqrt_fusion.2), kind=kOutput, calls=%fused_computation.50 | convolution fusion | flops 101892000 | bytes 1565440 | tf_op jit(solution)/shard_map/dot_general | solution.py:115
  30.3 8.7 %all_gather.31 = bf16[384,256]{1,0:T(8,128)(2,1)S(1)} all-gather(bf16[96,256]{1,0:T(8,128)(2,1)S(1)} %multiply_convert_fusion.1), channel_id=1, replica_groups=mesh['sp'=4,'tp'=4,'dp'=2] {'tp'}, dimensions={0}, use_global_device_ids=true | all-gather | bytes 245760 | tf_op jit(solution)/shard_map/all_gather | solution.py:126
  39.1 13.8 %all_gather.29 = bf16[512,256]{1,0:T(8,128)(2,1)S(1)} all-gather(bf16[128,256]{1,0:T(8,128)(2,1)S(1)} %copy-done.12), channel_id=1, replica_groups=mesh['sp'=4,'tp'=4,'dp'=2] {'sp'}, dimensions={0}, use_global_device_ids=true | all-gather | bytes 327680 | tf_op jit(solution)/shard_map/all_gather | solution.py:141
  52.9 0.9 convolution_convert_fusion.3
  54.0 1.0 convolution_convert_fusion
  56.0 8.5 %all_gather.28 = bf16[384,512]{1,0:T(8,128)(2,1)S(1)} all-gather(bf16[96,512]{1,0:T(8,128)(2,1)S(1)} %multiply_convert_fusion), channel_id=1, replica_groups=mesh['sp'=4,'tp'=4,'dp'=2] {'tp'}, dimensions={0}, use_global_device_ids=true | all-gather | bytes 491520 | tf_op jit(solution)/shard_map/all_gather | solution.py:125
  66.3 1.3 fusion.62
  69.6 0.9 fusion.47
  70.5 8.2 %all-gather = bf16[4,96,64]{1,2,0:T(8,128)(2,1)S(1)} all-gather(bf16[1,96,64]{1,2,0:T(8,128)(2,1)S(1)} %fusion.47), channel_id=1, replica_groups=mesh['sp'=4,'tp'=4,'dp'=2] {'tp'}, dimensions={0}, use_global_device_ids=true | all-gather | bytes 61440 | tf_op jit(solution)/shard_map/all_gather | solution.py:127
  79.4 1.6 reshape.254
  81.0 14.6 %all_gather.34 = bf16[1536,64]{0,1:T(8,128)(2,1)S(1)} all-gather(bf16[384,64]{0,1:T(8,128)(2,1)} %reshape.254), channel_id=1, replica_groups=mesh['sp'=4,'tp'=4,'dp'=2] {'sp'}, dimensions={0}, use_global_device_ids=true | all-gather | bytes 245760 | tf_op jit(solution)/shard_map/all_gather | solution.py:194
  95.6 16.9 %all_gather.32 = bf16[1536,256]{1,0:T(8,128)(2,1)S(1)} all-gather(bf16[384,256]{1,0:T(8,128)(2,1)} %convolution_convert_fusion.3), channel_id=1, replica_groups=mesh['sp'=4,'tp'=4,'dp'=2] {'sp'}, dimensions={0}, use_global_device_ids=true | all-gather | bytes 983040 | tf_op jit(solution)/shard_map/all_gather | solution.py:192
  112.9 12.2 %all_gather.30 = bf16[512,64]{0,1:T(8,128)(2,1)S(1)} all-gather(bf16[128,64]{0,1:T(8,128)(2,1)S(1)} %copy-done.13), channel_id=1, replica_groups=mesh['sp'=4,'tp'=4,'dp'=2] {'sp'}, dimensions={0}, use_global_device_ids=true | all-gather | bytes 81920 | tf_op jit(solution)/shard_map/all_gather | solution.py:142
  126.3 1.0 fusion.71
  128.3 15.6 %all_gather.35 = bf16[1536,256]{1,0:T(8,128)(2,1)S(1)} all-gather(bf16[384,256]{1,0:T(8,128)(2,1)S(1)} %convolution_convert_fusion.2), channel_id=1, replica_groups=mesh['sp'=4,'tp'=4,'dp'=2] {'sp'}, dimensions={0}, use_global_device_ids=true | all-gather | bytes 983040 | tf_op jit(solution)/shard_map/all_gather | solution.py:193
  145.5 0.9 fusion.23
  146.8 8.1 %all_to_all.19 = bf16[4,96,256]{2,1,0:T(8,128)(2,1)S(1)} all-to-all(bf16[4,96,256]{2,1,0:T(8,128)(2,1)S(1)} %all_to_all.14), channel_id=1, replica_groups=mesh['sp'=4,'tp'=4,'dp'=2] {'tp'}, dimensions={0} | all-to-all | bytes 393216 | tf_op jit(solution)/shard_map/all_to_all | solution.py:200
  154.9 3.8 %fusion.7 = bf16[96,2048]{1,0:T(8,128)(2,1)} fusion(bf16[96,1024]{1,0:T(8,128)(2,1)S(1)} %bitcast.116, bf16[1024,2048]{1,0:T(8,128)(2,1)} %param.35, bf16[96,2048]{1,0:T(8,128)(2,1)S(1)} %copy-done.1, f32[2048]{0:T(1024)S(1)} %bitcast.118), kind=kOutput, calls=%fused_computation.9 | convolution fusion | flops 403439616 | bytes 5185536 | tf_op jit(solution)/shard_map/dot_general | solution.py:201
  (80 shorter events, 11.5 us)
Async XLA Ops:
  0.0 55.3 %copy-start = (bf16[2048,512]{1,0:T(8,128)(2,1)S(1)}, bf16[2048,512]{1,0:T(8,128)(2,1)}, u32[]{:S(2)}) copy-start(bf16[2048,512]{1,0:T(8,128)(2,1)} %param.26) | copy-start | bytes 6291460
  0.0 30.2 %copy-start.19 = (f32[256]{0:T(256)S(1)}, f32[256]{0:T(256)}, u32[]{:S(2)}) copy-start(f32[256]{0:T(256)} %param.30) | copy-start | bytes 3076
  0.0 39.0 %copy-start.12 = (bf16[128,256]{1,0:T(8,128)(2,1)S(1)}, bf16[128,256]{1,0:T(8,128)(2,1)}, u32[]{:S(2)}) copy-start(bf16[128,256]{1,0:T(8,128)(2,1)} %param.20) | copy-start | bytes 196612
  1.3 51.5 %copy-start.3 = (bf16[256,256]{1,0:T(8,128)(2,1)S(1)}, bf16[256,256]{1,0:T(8,128)(2,1)}, u32[]{:S(2)}) copy-start(bf16[256,256]{1,0:T(8,128)(2,1)} %param.32) | copy-start | bytes 393220
  3.8 50.2 %copy-start.4 = (bf16[256,256]{1,0:T(8,128)(2,1)S(1)}, bf16[256,256]{1,0:T(8,128)(2,1)}, u32[]{:S(2)}) copy-start(bf16[256,256]{1,0:T(8,128)(2,1)} %param.33) | copy-start | bytes 393220
  27.1 28.1 %copy-start.14 = (f32[1,2048]{1,0:T(1,128)}, f32[1,2048]{1,0:T(1,128)S(1)}, u32[]{:S(2)}) copy-start(f32[1,2048]{1,0:T(1,128)S(1)} %get-tuple-element.15) | copy-start | bytes 24580
  27.1 27.9 %copy-start.5 = (bf16[256,256]{1,0:T(8,128)(2,1)S(1)}, bf16[256,256]{1,0:T(8,128)(2,1)}, u32[]{:S(2)}) copy-start(bf16[256,256]{1,0:T(8,128)(2,1)} %param.33) | copy-start | bytes 393220
  28.3 26.9 %copy-start.22 = (f32[96]{0:T(128)}, f32[96]{0:T(128)S(1)}, u32[]{:S(2)}) copy-start(f32[96]{0:T(128)S(1)} %add_rsqrt_fusion.2) | copy-start | bytes 1156
  28.3 26.9 %copy-start.1 = (bf16[96,2048]{1,0:T(8,128)(2,1)S(1)}, bf16[96,2048]{1,0:T(8,128)(2,1)}, u32[]{:S(2)}) copy-start(bf16[96,2048]{1,0:T(8,128)(2,1)} %param.18) | copy-start | bytes 1179652
  28.4 26.9 %copy-start.21 = (f32[2048]{0:T(1024)S(1)}, f32[2048]{0:T(1024)}, u32[]{:S(2)}) copy-start(f32[2048]{0:T(1024)} %param.25) | copy-start | bytes 24580
  53.7 2.2 %copy-start.17 = (f32[512]{0:T(512)S(1)}, f32[512]{0:T(512)}, u32[]{:S(2)}) copy-start(f32[512]{0:T(512)} %param.29) | copy-start | bytes 6148
  54.0 10.5 %copy-start.6 = (bf16[512,384]{1,0:T(8,128)(2,1)S(1)}, bf16[512,384]{1,0:T(8,128)(2,1)}, u32[]{:S(2)}) copy-start(bf16[512,384]{1,0:T(8,128)(2,1)} %param.31) | copy-start | bytes 1179652
  67.6 0.6 copy-start.11
  70.5 54.6 %copy-start.15 = (f32[384]{0:T(512)S(1)}, f32[384]{0:T(512)}, u32[]{:S(2)}) copy-start(f32[384]{0:T(512)} %get-tuple-element.33) | copy-start | bytes 4612
  70.5 54.6 %copy-start.16 = (f32[384]{0:T(512)S(1)}, f32[384]{0:T(512)}, u32[]{:S(2)}) copy-start(f32[384]{0:T(512)} %get-tuple-element.34) | copy-start | bytes 4612
  81.0 31.9 %copy-start.13 = (bf16[128,64]{0,1:T(8,128)(2,1)S(1)}, bf16[128,64]{0,1:T(8,128)(2,1)}, u32[]{:S(2)}) copy-start(bf16[128,64]{0,1:T(8,128)(2,1)} %param.21) | copy-start | bytes 49156
  81.0 44.1 %copy-start.18 = (f32[16]{0:T(128)S(1)}, f32[16]{0:T(128)}, u32[]{:S(2)}) copy-start(f32[16]{0:T(128)} %multiply_power_fusion) | copy-start | bytes 196
  81.0 44.4 %copy-start.7 = (f32[384,2,16]{0,2,1:T(8,128)S(1)}, f32[384,2,16]{0,2,1:T(8,128)}, u32[]{:S(2)}) copy-start(f32[384,2,16]{0,2,1:T(8,128)} %get-tuple-element.7) | copy-start | bytes 147460
  81.0 44.4 %copy-start.8 = (f32[384,2,16]{0,2,1:T(8,128)S(1)}, f32[384,2,16]{0,2,1:T(8,128)}, u32[]{:S(2)}) copy-start(f32[384,2,16]{0,2,1:T(8,128)} %get-tuple-element.8) | copy-start | bytes 147460
  81.0 44.4 %copy-start.9 = (f32[384,2,16]{0,2,1:T(8,128)S(1)}, f32[384,2,16]{0,2,1:T(8,128)}, u32[]{:S(2)}) copy-start(f32[384,2,16]{0,2,1:T(8,128)} %get-tuple-element.9) | copy-start | bytes 147460
  81.0 44.4 %copy-start.10 = (f32[384,2,16]{0,2,1:T(8,128)S(1)}, f32[384,2,16]{0,2,1:T(8,128)}, u32[]{:S(2)}) copy-start(f32[384,2,16]{0,2,1:T(8,128)} %get-tuple-element.10) | copy-start | bytes 147460
  126.3 1.0 copy-start.20
  143.8 1.0 copy-start.2
where the time goes:
time: 159 us
  blocking collectives  129 us (81%)
  matrix products  18.4 us (12%)
  other arithmetic  7.9 us (5%)
  local copies, waits for them, and re-layouts  3.43 us (2%)
    all_gather x1, blocking collectives, on_device(): lax.all_gather(own_nope, 'sp', axis=0, tiled=True)  16.9 us
    all_gather x1, blocking collectives, on_device(): lax.all_gather(own_values, 'sp', axis=0, tiled=True)  15.6 us
    all_gather x1, blocking collectives, on_device(): lax.all_gather(rope_group, 'sp', axis=0, tiled=True)  14.6 us
    all_gather x1, blocking collectives, on_device(): lax.all_gather(context_latent, 'sp', axis=0, tiled=True)  13.8 us
    psum x1, blocking collectives, on_device(): summed = lax.psum(partials, 'sp')  13.8 us
    all_gather x1, blocking collectives, on_device(): lax.all_gather(context_rope, 'sp', axis=0, tiled=True)  12.2 us
    all_gather x1, blocking collectives, on_device(): lax.all_gather(latent_low, 'tp', axis=0, tiled=True)  8.7 us
    all_gather x1, blocking collectives, on_device(): lax.all_gather(query_low, 'tp', axis=0, tiled=True)  8.53 us

commit v1 on v0

--- a/solution.py
+++ b/solution.py
@@ -100,7 +100,8 @@
         ]
     )
     summed = lax.psum(partials, "sp")
-    modulation = lax.all_gather(summed, "tp", axis=1, tiled=True)
+    blocks = lax.all_gather(summed, "tp")
+    modulation = jnp.concatenate(blocks, axis=1)
     shift_vec = modulation[0]
     scale_vec = modulation[1]
     gate_vec = modulation[2]

time: 159 us -> 159 us (level)
  no operation moved by 1% of the time
where the time goes in v1:
time: 159 us
  blocking collectives  129 us (81%)
  matrix products  18.4 us (12%)
  other arithmetic  7.9 us (5%)
  local copies, waits for them, and re-layouts  3.43 us (2%)
    all_gather x1, blocking collectives, on_device(): lax.all_gather(own_nope, 'sp', axis=0, tiled=True)  16.9 us
    all_gather x1, blocking collectives, on_device(): lax.all_gather(own_values, 'sp', axis=0, tiled=True)  15.6 us
    all_gather x1, blocking collectives, on_device(): lax.all_gather(rope_group, 'sp', axis=0, tiled=True)  14.6 us
    all_gather x1, blocking collectives, on_device(): lax.all_gather(context_latent, 'sp', axis=0, tiled=True)  13.8 us
    psum x1, blocking collectives, on_device(): summed = lax.psum(partials, 'sp')  13.8 us
    all_gather x1, blocking collectives, on_device(): lax.all_gather(context_rope, 'sp', axis=0, tiled=True)  12.2 us
    all_gather x1, blocking collectives, on_device(): lax.all_gather(latent_low, 'tp', axis=0, tiled=True)  8.7 us
    all_gather x1, blocking collectives, on_device(): lax.all_gather(query_low, 'tp', axis=0, tiled=True)  8.53 us

profile of v1, /device:TPU:0, one launch (start us, length us, event | category | flops | bytes accessed | tf_op | source)
XLA Modules:
  0.0 158.7 jit_solution(15833898411083995222)
XLA Ops:
  1.3 1.2 fusion.72
  2.6 1.2 fusion.73
  3.8 1.3 fusion.74
  5.1 13.8 %psum.7 = f32[1,3,512]{2,1,0:T(4,128)S(1)} all-reduce(f32[1,3,512]{2,1,0:T(4,128)S(1)} %maximum_bitcast_fusion), channel_id=1, replica_groups=mesh['sp'=4,'tp'=4,'dp'=2] {'sp'}, use_global_device_ids=true, to_apply=%region_0.1 | all-reduce | flops 1536 | bytes 12288 | tf_op jit(solution)/shard_map/psum | solution.py:102
  18.9 8.2 %all_gather.31 = f32[4,3,512]{2,1,0:T(4,128)S(1)} all-gather(f32[1,3,512]{2,1,0:T(4,128)S(1)} %psum.7), channel_id=1, replica_groups=mesh['sp'=4,'tp'=4,'dp'=2] {'tp'}, dimensions={0}, use_global_device_ids=true | all-gather | bytes 30720 | tf_op jit(solution)/shard_map/all_gather | solution.py:103
  27.1 1.2 fusion.26
  28.4 1.9 %multiply_reduce_fusion.1 = (f32[96]{0:T(128)S(1)}, f32[96,256]{1,0:T(8,128)S(1)}) fusion(bf16[2048,256]{1,0:T(8,128)(2,1)} %param.27, bf16[96,2048]{1,0:T(8,128)(2,1)} %param.18, f32[2048]{0:T(1024)S(1)} %bitcast.123, f32[2048]{0:T(1024)S(1)} %bitcast.126, f32[2048]{0:T(1024)} %param.25, f32[96]{0:T(128)S(1)} %add_rsqrt_fusion.2), kind=kOutput, calls=%fused_computation.50 | convolution fusion | flops 101892000 | bytes 1565440 | tf_op jit(solution)/shard_map/dot_general | solution.py:116
  30.3 8.7 %all_gather.35 = bf16[384,256]{1,0:T(8,128)(2,1)S(1)} all-gather(bf16[96,256]{1,0:T(8,128)(2,1)S(1)} %multiply_convert_fusion.1), channel_id=1, replica_groups=mesh['sp'=4,'tp'=4,'dp'=2] {'tp'}, dimensions={0}, use_global_device_ids=true | all-gather | bytes 245760 | tf_op jit(solution)/shard_map/all_gather | solution.py:127
  39.1 13.8 %all_gather.33 = bf16[512,256]{1,0:T(8,128)(2,1)S(1)} all-gather(bf16[128,256]{1,0:T(8,128)(2,1)S(1)} %copy-done.12), channel_id=1, replica_groups=mesh['sp'=4,'tp'=4,'dp'=2] {'sp'}, dimensions={0}, use_global_device_ids=true | all-gather | bytes 327680 | tf_op jit(solution)/shard_map/all_gather | solution.py:142
  52.9 0.9 convolution_convert_fusion.3
  54.0 1.0 convolution_convert_fusion
  56.0 8.5 %all_gather.32 = bf16[384,512]{1,0:T(8,128)(2,1)S(1)} all-gather(bf16[96,512]{1,0:T(8,128)(2,1)S(1)} %multiply_convert_fusion), channel_id=1, replica_groups=mesh['sp'=4,'tp'=4,'dp'=2] {'tp'}, dimensions={0}, use_global_device_ids=true | all-gather | bytes 491520 | tf_op jit(solution)/shard_map/all_gather | solution.py:126
  66.3 1.3 fusion.62
  69.6 0.9 fusion.47
  70.5 8.2 %all-gather = bf16[4,96,64]{1,2,0:T(8,128)(2,1)S(1)} all-gather(bf16[1,96,64]{1,2,0:T(8,128)(2,1)S(1)} %fusion.47), channel_id=1, replica_groups=mesh['sp'=4,'tp'=4,'dp'=2] {'tp'}, dimensions={0}, use_global_device_ids=true | all-gather | bytes 61440 | tf_op jit(solution)/shard_map/all_gather | solution.py:128
  79.4 1.6 reshape.272
  81.0 14.6 %all_gather.38 = bf16[1536,64]{0,1:T(8,128)(2,1)S(1)} all-gather(bf16[384,64]{0,1:T(8,128)(2,1)} %reshape.272), channel_id=1, replica_groups=mesh['sp'=4,'tp'=4,'dp'=2] {'sp'}, dimensions={0}, use_global_device_ids=true | all-gather | bytes 245760 | tf_op jit(solution)/shard_map/all_gather | solution.py:195
  95.6 16.9 %all_gather.36 = bf16[1536,256]{1,0:T(8,128)(2,1)S(1)} all-gather(bf16[384,256]{1,0:T(8,128)(2,1)} %convolution_convert_fusion.3), channel_id=1, replica_groups=mesh['sp'=4,'tp'=4,'dp'=2] {'sp'}, dimensions={0}, use_global_device_ids=true | all-gather | bytes 983040 | tf_op jit(solution)/shard_map/all_gather | solution.py:193
  112.9 12.2 %all_gather.34 = bf16[512,64]{0,1:T(8,128)(2,1)S(1)} all-gather(bf16[128,64]{0,1:T(8,128)(2,1)S(1)} %copy-done.13), channel_id=1, replica_groups=mesh['sp'=4,'tp'=4,'dp'=2] {'sp'}, dimensions={0}, use_global_device_ids=true | all-gather | bytes 81920 | tf_op jit(solution)/shard_map/all_gather | solution.py:143
  126.3 1.0 fusion.71
  128.3 15.6 %all_gather.39 = bf16[1536,256]{1,0:T(8,128)(2,1)S(1)} all-gather(bf16[384,256]{1,0:T(8,128)(2,1)S(1)} %convolution_convert_fusion.2), channel_id=1, replica_groups=mesh['sp'=4,'tp'=4,'dp'=2] {'sp'}, dimensions={0}, use_global_device_ids=true | all-gather | bytes 983040 | tf_op jit(solution)/shard_map/all_gather | solution.py:194
  145.5 0.9 fusion.23
  146.8 8.1 %all_to_all.19 = bf16[4,96,256]{2,1,0:T(8,128)(2,1)S(1)} all-to-all(bf16[4,96,256]{2,1,0:T(8,128)(2,1)S(1)} %all_to_all.14), channel_id=1, replica_groups=mesh['sp'=4,'tp'=4,'dp'=2] {'tp'}, dimensions={0} | all-to-all | bytes 393216 | tf_op jit(solution)/shard_map/all_to_all | solution.py:201
  154.9 3.8 %fusion.7 = bf16[96,2048]{1,0:T(8,128)(2,1)} fusion(bf16[96,1024]{1,0:T(8,128)(2,1)S(1)} %bitcast.119, bf16[1024,2048]{1,0:T(8,128)(2,1)} %param.35, bf16[96,2048]{1,0:T(8,128)(2,1)S(1)} %copy-done.1, f32[2048]{0:T(1024)S(1)} %bitcast.122), kind=kOutput, calls=%fused_computation.9 | convolution fusion | flops 403439616 | bytes 5185536 | tf_op jit(solution)/shard_map/dot_general | solution.py:202
  (80 shorter events, 11.6 us)
Async XLA Ops:
  0.0 55.3 %copy-start = (bf16[2048,512]{1,0:T(8,128)(2,1)S(1)}, bf16[2048,512]{1,0:T(8,128)(2,1)}, u32[]{:S(2)}) copy-start(bf16[2048,512]{1,0:T(8,128)(2,1)} %param.26) | copy-start | bytes 6291460
  0.0 30.2 %copy-start.19 = (f32[256]{0:T(256)S(1)}, f32[256]{0:T(256)}, u32[]{:S(2)}) copy-start(f32[256]{0:T(256)} %param.30) | copy-start | bytes 3076
  0.0 39.0 %copy-start.12 = (bf16[128,256]{1,0:T(8,128)(2,1)S(1)}, bf16[128,256]{1,0:T(8,128)(2,1)}, u32[]{:S(2)}) copy-start(bf16[128,256]{1,0:T(8,128)(2,1)} %param.20) | copy-start | bytes 196612
  1.3 51.5 %copy-start.3 = (bf16[256,256]{1,0:T(8,128)(2,1)S(1)}, bf16[256,256]{1,0:T(8,128)(2,1)}, u32[]{:S(2)}) copy-start(bf16[256,256]{1,0:T(8,128)(2,1)} %param.32) | copy-start | bytes 393220
  3.8 50.2 %copy-start.4 = (bf16[256,256]{1,0:T(8,128)(2,1)S(1)}, bf16[256,256]{1,0:T(8,128)(2,1)}, u32[]{:S(2)}) copy-start(bf16[256,256]{1,0:T(8,128)(2,1)} %param.33) | copy-start | bytes 393220
  27.1 28.1 %copy-start.14 = (f32[1,4,512]{2,0,1:T(1,128)}, f32[1,4,512]{2,0,1:T(1,128)S(1)}, u32[]{:S(2)}) copy-start(f32[1,4,512]{2,0,1:T(1,128)S(1)} %get-tuple-element.15) | copy-start | bytes 24580
  27.1 27.9 %copy-start.5 = (bf16[256,256]{1,0:T(8,128)(2,1)S(1)}, bf16[256,256]{1,0:T(8,128)(2,1)}, u32[]{:S(2)}) copy-start(bf16[256,256]{1,0:T(8,128)(2,1)} %param.33) | copy-start | bytes 393220
  28.3 26.9 %copy-start.22 = (f32[96]{0:T(128)}, f32[96]{0:T(128)S(1)}, u32[]{:S(2)}) copy-start(f32[96]{0:T(128)S(1)} %add_rsqrt_fusion.2) | copy-start | bytes 1156
  28.3 26.9 %copy-start.1 = (bf16[96,2048]{1,0:T(8,128)(2,1)S(1)}, bf16[96,2048]{1,0:T(8,128)(2,1)}, u32[]{:S(2)}) copy-start(bf16[96,2048]{1,0:T(8,128)(2,1)} %param.18) | copy-start | bytes 1179652
  28.4 26.9 %copy-start.21 = (f32[2048]{0:T(1024)S(1)}, f32[2048]{0:T(1024)}, u32[]{:S(2)}) copy-start(f32[2048]{0:T(1024)} %param.25) | copy-start | bytes 24580
  53.7 2.2 %copy-start.17 = (f32[512]{0:T(512)S(1)}, f32[512]{0:T(512)}, u32[]{:S(2)}) copy-start(f32[512]{0:T(512)} %param.29) | copy-start | bytes 6148
  54.0 10.5 %copy-start.6 = (bf16[512,384]{1,0:T(8,128)(2,1)S(1)}, bf16[512,384]{1,0:T(8,128)(2,1)}, u32[]{:S(2)}) copy-start(bf16[512,384]{1,0:T(8,128)(2,1)} %param.31) | copy-start | bytes 1179652
  67.6 0.6 copy-start.11
  70.5 54.6 %copy-start.15 = (f32[384]{0:T(512)S(1)}, f32[384]{0:T(512)}, u32[]{:S(2)}) copy-start(f32[384]{0:T(512)} %get-tuple-element.33) | copy-start | bytes 4612
  70.5 54.6 %copy-start.16 = (f32[384]{0:T(512)S(1)}, f32[384]{0:T(512)}, u32[]{:S(2)}) copy-start(f32[384]{0:T(512)} %get-tuple-element.34) | copy-start | bytes 4612
  81.0 31.9 %copy-start.13 = (bf16[128,64]{0,1:T(8,128)(2,1)S(1)}, bf16[128,64]{0,1:T(8,128)(2,1)}, u32[]{:S(2)}) copy-start(bf16[128,64]{0,1:T(8,128)(2,1)} %param.21) | copy-start | bytes 49156
  81.0 44.1 %copy-start.18 = (f32[16]{0:T(128)S(1)}, f32[16]{0:T(128)}, u32[]{:S(2)}) copy-start(f32[16]{0:T(128)} %multiply_power_fusion) | copy-start | bytes 196
  81.0 44.4 %copy-start.7 = (f32[384,2,16]{0,2,1:T(8,128)S(1)}, f32[384,2,16]{0,2,1:T(8,128)}, u32[]{:S(2)}) copy-start(f32[384,2,16]{0,2,1:T(8,128)} %get-tuple-element.7) | copy-start | bytes 147460
  81.0 44.4 %copy-start.8 = (f32[384,2,16]{0,2,1:T(8,128)S(1)}, f32[384,2,16]{0,2,1:T(8,128)}, u32[]{:S(2)}) copy-start(f32[384,2,16]{0,2,1:T(8,128)} %get-tuple-element.8) | copy-start | bytes 147460
  81.0 44.4 %copy-start.9 = (f32[384,2,16]{0,2,1:T(8,128)S(1)}, f32[384,2,16]{0,2,1:T(8,128)}, u32[]{:S(2)}) copy-start(f32[384,2,16]{0,2,1:T(8,128)} %get-tuple-element.9) | copy-start | bytes 147460
  81.0 44.4 %copy-start.10 = (f32[384,2,16]{0,2,1:T(8,128)S(1)}, f32[384,2,16]{0,2,1:T(8,128)}, u32[]{:S(2)}) copy-start(f32[384,2,16]{0,2,1:T(8,128)} %get-tuple-element.10) | copy-start | bytes 147460
  126.3 1.0 copy-start.20
  143.9 1.0 copy-start.2
